TPU v7x, 32 devices: a whole 2x2x4 slice. The times are simulated.
32 devices in a mesh: grp: 2 (over y), tp: 4 (over z), dp: 4 (over x, core).
Axes of the slice: x: 2, y: 2, z: 4, core: 2. Of those that a mesh axis runs over, the one named last changes fastest.
Arguments:
- tokens: bfloat16 [128, 8, 2048], P('grp', None, 'dp'), parts along dimension 0, may hold values from -64 to 64
- live_counts: int32 [128], P(('grp', 'dp')), parts along dimension 0, may hold values from 1 to 8, 256 in all
- norm_gain: float32 [2, 2048], P(None, 'dp'), may hold values from 0.1 to 1.9
- w_branch: bfloat16 [2, 2048, 4096], P(None, 'dp', 'tp'), may hold values from -0.125 to 0.125
- w_silu_gate: bfloat16 [2, 2048, 4096], P(None, 'dp', 'tp'), may hold values from -0.125 to 0.125
- conv_weight: float32 [2, 4, 4096], P(None, None, 'tp'), may hold values from -3 to 3
- w_query: bfloat16 [2, 16, 256, 256], P(None, 'tp'), may hold values from -0.375 to 0.375
- w_key: bfloat16 [2, 16, 256, 256], P(None, 'tp'), may hold values from -0.375 to 0.375
- w_value: bfloat16 [2, 16, 256, 256], P(None, 'tp'), may hold values from -0.375 to 0.375
- w_input_gate: bfloat16 [2, 16, 768], P(None, 'tp'), may hold values from -0.21875 to 0.21875
- w_forget_gate: bfloat16 [2, 16, 768], P(None, 'tp'), may hold values from -0.21875 to 0.21875
- bias_input: float32 [2, 16], P(None, 'tp'), may hold values from -2 to 2
- bias_forget: float32 [2, 16], P(None, 'tp'), may hold values from -1 to 5
- out_gain: float32 [2, 16, 256], P(None, 'tp'), may hold values from 0.25 to 4
- skip_gain: float32 [2, 4096], P(None, 'tp'), may hold values from 0.25 to 4
- w_out: bfloat16 [2, 4096, 2048], P(None, 'tp', 'dp'), may hold values from -0.09375 to 0.09375
- conv_state: bfloat16 [2, 128, 3, 4096], P(None, ('grp', 'dp'), None, 'tp'), parts along dimension 1, may hold values from -6 to 6
- memory: float32 [2, 128, 16, 256, 256], P(None, ('grp', 'dp'), 'tp'), parts along dimension 1, may hold values from -0.375 to 0.375
- max_state: float32 [2, 128, 16], P(None, ('grp', 'dp'), 'tp'), parts along dimension 1, may hold values from -4 to 4
Outputs:
- out_tokens: bfloat16 [128, 8, 2048], P('grp', None, 'dp'), parts along dimension 0
- new_conv_state: bfloat16 [2, 128, 3, 4096], P(None, ('grp', 'dp'), None, 'tp'), parts along dimension 1
- new_memory: float32 [2, 128, 16, 256, 256], P(None, ('grp', 'dp'), 'tp'), parts along dimension 1
- new_max: float32 [2, 128, 16], P(None, ('grp', 'dp'), 'tp'), parts along dimension 1
There are 2 independent parts, one for each index of `grp`. A program takes and returns all parts, laid end to end along the dimension named above; an argument that names none is the same for every part. Nothing has to cross between parts.
Inputs may be any that keep to these rules, and one draw needn't show every extreme that they name: `live_counts`: each sequence has at least one live slot; within each part (each independent copy of the problem) the 64 counts sum to 256, so the whole array sums to that times the number of parts; in each part some sequence uses all 8 slots.
All inputs are finite; a program needn't handle non-finite values. No bound on the sum of `live_counts` on one device may be relied on, other than what follows from the above.
Results may differ from a plain program's by a relative error of at most 0.035.
Values may be sent and summed in bfloat16 or wider, within the bound.
A program may use at most 192 MiB of HBM per device.

v0:
```python
import jax
import jax.numpy as jnp
from jax import lax
from jax.sharding import PartitionSpec as P

D = 2048
HEAD_DIM = 256
CONV = 4
LAYERS = 2
epsilon = 1e-06
very_negative = -1e30


def recurrent_cell(
    branch,
    silu_gate,
    live_counts,
    conv_weight,
    w_query,
    w_key,
    w_value,
    w_input_gate,
    w_forget_gate,
    bias_input,
    bias_forget,
    out_gain,
    skip_gain,
    conv_state,
    memory,
    max_state,
):
    local_batch = branch.shape[0]
    steps = branch.shape[1]
    local_width = branch.shape[2]
    local_heads = w_query.shape[0]
    padded = jnp.concatenate([conv_state, branch], axis=1)
    conv_sum = jnp.zeros((local_batch, steps, local_width), jnp.float32)
    for offset in range(CONV):
        conv_sum = (
            conv_sum + padded[:, offset : offset + steps].astype(jnp.float32) * conv_weight[offset]
        )
    convolved = jax.nn.silu(conv_sum).astype(jnp.bfloat16)
    picks = live_counts[:, None] + jnp.arange(CONV - 1, dtype=jnp.int32)[None, :]
    new_conv = jnp.take_along_axis(padded, picks[:, :, None], axis=1)
    conv_heads = convolved.reshape(local_batch, steps, local_heads, HEAD_DIM)
    branch_heads = branch.reshape(local_batch, steps, local_heads, HEAD_DIM)
    queries = jnp.einsum(
        "blhd,hde->blhe", conv_heads, w_query, preferred_element_type=jnp.float32
    ).astype(jnp.bfloat16)
    key_rows = jnp.einsum(
        "blhd,hde->blhe", conv_heads, w_key, preferred_element_type=jnp.float32
    ).astype(jnp.bfloat16)
    value_rows = jnp.einsum(
        "blhd,hde->blhe", branch_heads, w_value, preferred_element_type=jnp.float32
    ).astype(jnp.bfloat16)
    joined = jnp.concatenate([queries, key_rows, value_rows], axis=-1)
    input_log = (
        jnp.einsum("blhc,hc->blh", joined, w_input_gate, preferred_element_type=jnp.float32)
        + bias_input
    )
    forget_pre = (
        jnp.einsum("blhc,hc->blh", joined, w_forget_gate, preferred_element_type=jnp.float32)
        + bias_forget
    )
    forget_log = jax.nn.log_sigmoid(forget_pre)
    positions = jnp.arange(steps, dtype=jnp.int32)
    live = positions[None, :] < live_counts[:, None]
    input_log = jnp.transpose(jnp.where(live[:, :, None], input_log, very_negative), (0, 2, 1))
    forget_log = jnp.transpose(jnp.where(live[:, :, None], forget_log, 0.0), (0, 2, 1))
    query_heads = jnp.transpose(queries.astype(jnp.float32), (0, 2, 1, 3))
    key_heads = jnp.transpose(key_rows.astype(jnp.float32), (0, 2, 1, 3)) * HEAD_DIM ** (-0.5)
    value_heads = jnp.transpose(value_rows.astype(jnp.float32), (0, 2, 1, 3))
    cumulative = jnp.cumsum(forget_log, axis=-1)
    log_weights = cumulative[..., :, None] - cumulative[..., None, :] + input_log[..., None, :]
    causal = positions[:, None] >= positions[None, :]
    log_weights = jnp.where(causal, log_weights, very_negative)
    carried = cumulative + max_state[..., None]
    stabilizer = jnp.maximum(jnp.max(log_weights, axis=-1), carried)
    weights = jnp.exp(log_weights - stabilizer[..., None])
    carried_scale = jnp.exp(carried - stabilizer)
    scores = jnp.einsum("bhtd,bhsd->bhts", query_heads, key_heads) * weights
    numerator = jnp.einsum("bhts,bhse->bhte", scores, value_heads)
    numerator = numerator + carried_scale[..., None] * jnp.einsum(
        "bhtd,bhde->bhte", query_heads, memory
    )
    centered = numerator - jnp.mean(numerator, axis=-1, keepdims=True)
    normalized = centered * lax.rsqrt(
        jnp.mean(centered * centered, axis=-1, keepdims=True) + epsilon
    )
    normalized = normalized * out_gain[None, :, None, :]
    readout = jnp.transpose(normalized, (0, 2, 1, 3)).reshape(local_batch, steps, local_width)
    new_max = stabilizer[..., -1]
    decay = jnp.exp(cumulative[..., -1] + max_state - new_max)
    update_weight = jnp.exp(cumulative[..., -1:] - cumulative + input_log - new_max[..., None])
    new_memory = decay[..., None, None] * memory + jnp.einsum(
        "bhs,bhsd,bhse->bhde", update_weight, key_heads, value_heads
    )
    mixed = (readout + skip_gain * convolved.astype(jnp.float32)) * jax.nn.silu(
        silu_gate.astype(jnp.float32)
    )
    mixed = jnp.where(live[:, :, None], mixed, 0.0).astype(jnp.bfloat16)
    return (mixed, new_conv, new_memory, new_max)


def layer_step(
    tokens,
    live_counts,
    gain,
    w_branch,
    w_silu_gate,
    conv_weight,
    w_query,
    w_key,
    w_value,
    w_input_gate,
    w_forget_gate,
    bias_input,
    bias_forget,
    out_gain,
    skip_gain,
    w_out,
    conv_state,
    memory,
    max_state,
):
    all_batch = tokens.shape[0]
    steps = tokens.shape[1]
    local_features = tokens.shape[2]
    local_width = w_branch.shape[1]
    local_batch = live_counts.shape[0]
    floats = tokens.astype(jnp.float32)
    partial_squares = jnp.sum(floats * floats, axis=-1)
    total_squares = lax.psum(partial_squares, "dp")
    normed = (floats * lax.rsqrt(total_squares / D + epsilon)[..., None] * gain).astype(
        jnp.bfloat16
    )
    rows = normed.reshape(local_batch * lax.axis_size("dp") * steps, local_features)
    first = jnp.dot(rows, w_branch, preferred_element_type=jnp.float32)
    second = jnp.dot(rows, w_silu_gate, preferred_element_type=jnp.float32)
    summed = lax.psum_scatter(
        jnp.stack([first, second], axis=1)
        .reshape(local_batch * lax.axis_size("dp"), steps, 2, local_width)
        .astype(jnp.bfloat16),
        "dp",
        scatter_dimension=0,
        tiled=True,
    ).astype(jnp.float32)
    branch = summed[:, :, 0].astype(jnp.bfloat16)
    silu_gate = summed[:, :, 1].astype(jnp.bfloat16)
    mixed, new_conv, new_memory, new_max = recurrent_cell(
        branch,
        silu_gate,
        live_counts,
        conv_weight,
        w_query,
        w_key,
        w_value,
        w_input_gate,
        w_forget_gate,
        bias_input,
        bias_forget,
        out_gain,
        skip_gain,
        conv_state,
        memory,
        max_state,
    )
    piece = lax.all_gather(mixed, "dp", axis=0, tiled=True)
    flat = piece.reshape(piece.shape[0] * steps, local_width)
    product = jnp.dot(flat, w_out, preferred_element_type=jnp.float32)
    terms = product.reshape(piece.shape[0], steps, local_features)
    flat_terms = terms.reshape(all_batch * steps, local_features)
    share = lax.psum_scatter(
        flat_terms.astype(jnp.bfloat16), "tp", scatter_dimension=0, tiled=True
    ).astype(jnp.float32)
    share_rows = share.shape[0]
    residual_rows = lax.dynamic_slice_in_dim(
        floats.reshape(all_batch * steps, local_features),
        lax.axis_index("tp") * share_rows,
        share_rows,
        0,
    )
    new_share = (residual_rows + share.astype(jnp.bfloat16).astype(jnp.float32)).astype(
        jnp.bfloat16
    )
    result = lax.all_gather(new_share, "tp", axis=0, tiled=True).reshape(
        all_batch, steps, local_features
    )
    return (result, new_conv, new_memory, new_max)


def per_device(
    tokens,
    live_counts,
    norm_gain,
    w_branch,
    w_silu_gate,
    conv_weight,
    w_query,
    w_key,
    w_value,
    w_input_gate,
    w_forget_gate,
    bias_input,
    bias_forget,
    out_gain,
    skip_gain,
    w_out,
    conv_state,
    memory,
    max_state,
):
    stream = tokens
    conv_list = []
    memory_list = []
    max_list = []
    for which_layer in range(LAYERS):
        stream, new_conv, new_memory, new_max = layer_step(
            stream,
            live_counts,
            norm_gain[which_layer],
            w_branch[which_layer],
            w_silu_gate[which_layer],
            conv_weight[which_layer],
            w_query[which_layer],
            w_key[which_layer],
            w_value[which_layer],
            w_input_gate[which_layer],
            w_forget_gate[which_layer],
            bias_input[which_layer],
            bias_forget[which_layer],
            out_gain[which_layer],
            skip_gain[which_layer],
            w_out[which_layer],
            conv_state[which_layer],
            memory[which_layer],
            max_state[which_layer],
        )
        conv_list.append(new_conv)
        memory_list.append(new_memory)
        max_list.append(new_max)
    return (stream, jnp.stack(conv_list), jnp.stack(memory_list), jnp.stack(max_list))


def solution(mesh):
    in_specs = (
        P("grp", None, "dp"),
        P(("grp", "dp")),
        P(None, "dp"),
        P(None, "dp", "tp"),
        P(None, "dp", "tp"),
        P(None, None, "tp"),
        P(None, "tp", None, None),
        P(None, "tp", None, None),
        P(None, "tp", None, None),
        P(None, "tp", None),
        P(None, "tp", None),
        P(None, "tp"),
        P(None, "tp"),
        P(None, "tp", None),
        P(None, "tp"),
        P(None, "tp", "dp"),
        P(None, ("grp", "dp"), None, "tp"),
        P(None, ("grp", "dp"), "tp", None, None),
        P(None, ("grp", "dp"), "tp"),
    )
    out_specs = (
        P("grp", None, "dp"),
        P(None, ("grp", "dp"), None, "tp"),
        P(None, ("grp", "dp"), "tp", None, None),
        P(None, ("grp", "dp"), "tp"),
    )
    return jax.shard_map(
        per_device, mesh=mesh, in_specs=in_specs, out_specs=out_specs, check_vma=False
    )
```

profile of v0, /device:TPU:0, one launch (start us, length us, event | category | flops | bytes accessed | tf_op | source)
XLA Modules:
  0.0 297.1 jit_solution(8914190688373300822)
XLA Ops:
  7.2 1.4 fusion.162
  8.7 1.2 fusion.16
  9.9 12.9 %psum.14 = f32[64,8]{1,0:T(8,128)S(1)} all-reduce(f32[64,8]{1,0:T(8,128)S(1)} %fusion.16), channel_id=1, replica_groups=mesh['grp'=2,'tp'=4,'dp'=4] {'dp'}, use_global_device_ids=true, to_apply=%region_1.0 | all-reduce | flops 512 | bytes 4096 | tf_op jit(solution)/shard_map/psum | solution.py:133
  22.8 2.1 fusion.11
  26.2 2.5 copy.279
  34.3 26.1 %reduce-scatter.15.cloned.1.call-done = bf16[16,16384]{1,0:T(8,128)(2,1)} async-done(((bf16[64,16384]{1,0:T(8,128)(2,1)}), bf16[16,16384]{1,0:T(8,128)(2,1)}) %reduce-scatter.15.cloned.1.call-update) | async-done | bytes 524304
  60.5 1.4 copy.280
  62.1 0.9 reshape.308
  63.7 1.4 convolution_convert_fusion.10
  65.6 1.8 fusion.76
  67.4 1.8 fusion.77
  69.4 2.8 reduce_window_sum.17
  73.6 0.8 exponential_multiply_fusion.1
  74.4 0.8 bitcast_multiply_fusion.6
  75.2 7.0 %fusion.4 = f32[16,4,8,256]{3,2,1,0:T(8,128)S(1)} fusion(f32[2,16,4,256,256]{4,3,2,1,0:T(8,128)} %param.38, bf16[4,16,8,256]{3,2,1,0:T(8,128)(2,1)S(1)} %convolution_convert_fusion.11), kind=kOutput, calls=%fused_computation.9 | convolution fusion | flops 67108864 | bytes 9175040 | tf_op jit(solution)/shard_map/bhtd,bhde->bhte/dot_general | solution.py:83
  82.2 1.4 fusion.108
  84.8 0.9 copy.214
  85.8 16.8 %all-gather.3.cloned.1.call-done = bf16[64,8,1024]{2,1,0:T(8,128)(2,1)} async-done(((bf16[16,8,1024]{2,1,0:T(8,128)(2,1)}), bf16[64,8,1024]{2,1,0:T(8,128)(2,1)}) %all-gather.3.cloned.1.call-update) | async-done | bytes 1048592 | tf_op jit(solution)/shard_map/all_gather | solution.py:168
  102.6 3.0 %convolution_convert_fusion.5 = bf16[512,512]{1,0:T(8,128)(2,1)} fusion(bf16[64,8,1024]{2,1,0:T(8,128)(2,1)} %all-gather.3.cloned.1.call-done, bf16[2,1024,512]{2,1,0:T(8,128)(2,1)} %param.36), kind=kOutput, calls=%fused_computation.29 | convolution fusion | flops 537133056 | bytes 2621440 | tf_op jit(solution)/shard_map/dot_general | solution.py:170
  105.8 21.8 %reduce-scatter.11.cloned.1.call-done = bf16[128,512]{1,0:T(8,128)(2,1)} async-done(((bf16[512,512]{1,0:T(8,128)(2,1)}), bf16[128,512]{1,0:T(8,128)(2,1)}) %reduce-scatter.11.cloned.1.call-update) | async-done | bytes 131088 | tf_op jit(solution)/shard_map/reduce_scatter | solution.py:173
  127.6 0.9 add_convert_fusion.1
  128.6 15.6 %all_gather.13 = bf16[512,512]{1,0:T(8,128)(2,1)S(1)} all-gather(bf16[128,512]{1,0:T(8,128)(2,1)S(1)} %add_convert_fusion.1), channel_id=1, replica_groups=mesh['grp'=2,'tp'=4,'dp'=4] {'tp'}, dimensions={0}, use_global_device_ids=true | all-gather | bytes 655360 | tf_op jit(solution)/shard_map/all_gather | solution.py:186
  144.4 10.3 %psum.15 = f32[64,8]{1,0:T(8,128)S(1)} all-reduce(f32[64,8]{1,0:T(8,128)S(1)} %reduce_sum.60), channel_id=1, replica_groups=mesh['grp'=2,'tp'=4,'dp'=4] {'dp'}, use_global_device_ids=true, to_apply=%region_9.10 | all-reduce | flops 512 | bytes 4096 | tf_op jit(solution)/shard_map/psum | solution.py:133
  154.8 2.0 fusion.13
  156.8 2.0 fusion.12
  159.2 2.5 copy.281
  163.5 28.2 %reduce-scatter.17.cloned.1.call-done = bf16[16,16384]{1,0:T(8,128)(2,1)} async-done(((bf16[64,16384]{1,0:T(8,128)(2,1)}), bf16[16,16384]{1,0:T(8,128)(2,1)}) %reduce-scatter.17.cloned.1.call-update) | async-done | bytes 524304
  191.6 1.4 copy.282
  193.9 0.9 reshape.309
  195.3 1.4 convolution_convert_fusion.8
  196.8 1.4 convolution_convert_fusion.7
  198.2 1.5 convolution_convert_fusion.6
  199.8 1.8 fusion.74
  201.6 1.8 fusion.75
  203.6 2.8 reduce_window_sum.18
  207.1 7.1 %fusion = f32[16,4,8,256]{3,2,1,0:T(8,128)S(1)} fusion(f32[2,16,4,256,256]{4,3,2,1,0:T(8,128)} %param.38, bf16[4,16,8,256]{3,2,1,0:T(8,128)(2,1)} %copy-done.1), kind=kOutput, calls=%fused_computation.4 | convolution fusion | flops 67108864 | bytes 9175040 | tf_op jit(solution)/shard_map/bhtd,bhde->bhte/dot_general | solution.py:83
  214.2 1.2 gather_fusion
  215.4 1.2 gather_fusion.1
  218.7 1.7 bitcast_multiply_fusion.3
  220.4 1.5 fusion.109
  223.4 0.9 copy.227
  225.1 10.8 %fusion.3 = f32[1,16,4,256,256]{4,3,2,1,0:T(8,128)} fusion(f32[2,16,4,256,256]{4,3,2,1,0:T(8,128)} %param.38, f32[16,4]{1,0:T(8,128)S(1)} %copy.242, bf16[16,4,8,256]{3,2,0,1:T(8,128)(2,1)S(1)} %get-tuple-element.27, bf16[4,16,8,256]{3,2,1,0:T(8,128)(2,1)S(1)} %copy-done.9), kind=kOutput, calls=%fused_computation.7 | convolution fusion | flops 75497472 | bytes 34078976 | tf_op jit(solution)/shard_map/bhs,bhsd,bhse->bhde/dot_general | solution.py:95
  236.0 10.8 %fusion.7 = f32[1,16,4,256,256]{4,3,2,1,0:T(8,128)} fusion(f32[2,16,4,256,256]{4,3,2,1,0:T(8,128)} %param.38, f32[16,4]{1,0:T(8,128)S(1)} %copy.234, bf16[16,4,8,256]{3,2,0,1:T(8,128)(2,1)S(1)} %get-tuple-element.25, bf16[4,16,8,256]{3,2,1,0:T(8,128)(2,1)S(1)} %copy-done.7), kind=kOutput, calls=%fused_computation.12 | convolution fusion | flops 75497472 | bytes 34078976 | tf_op jit(solution)/shard_map/bhs,bhsd,bhse->bhde/dot_general | solution.py:95
  246.8 3.0 %convolution_convert_fusion.4 = bf16[512,512]{1,0:T(8,128)(2,1)} fusion(bf16[64,8,1024]{2,1,0:T(8,128)(2,1)} %all-gather.5.cloned.1.call-done, bf16[2,1024,512]{2,1,0:T(8,128)(2,1)} %param.36), kind=kOutput, calls=%fused_computation.28 | convolution fusion | flops 537133056 | bytes 2621440 | tf_op jit(solution)/shard_map/dot_general | solution.py:170
  249.9 23.1 %pad_maximum_fusion = f32[2,16,4,256,256]{4,3,2,1,0:T(8,128)} fusion(f32[1,16,4,256,256]{4,3,2,1,0:T(8,128)} %fusion.3, f32[1,16,4,256,256]{4,3,2,1,0:T(8,128)} %fusion.7), kind=kLoop, calls=%fused_computation.2 | loop fusion | flops 8388608 | bytes 67108864 | tf_op jit(solution)/shard_map/stack | solution.py:242
  273.0 0.9 add_convert_fusion
  273.9 15.6 %all_gather.15 = bf16[512,512]{1,0:T(8,128)(2,1)S(1)} all-gather(bf16[128,512]{1,0:T(8,128)(2,1)S(1)} %add_convert_fusion), channel_id=1, replica_groups=mesh['grp'=2,'tp'=4,'dp'=4] {'tp'}, dimensions={0}, use_global_device_ids=true | all-gather | bytes 655360 | tf_op jit(solution)/shard_map/all_gather | solution.py:186
  289.5 0.8 copy.380
  (200 shorter events, 20.1 us)
Async XLA Ops:
  7.2 17.8 %copy-start = (bf16[64,8,512]{2,1,0:T(8,128)(2,1)S(1)}, bf16[64,8,512]{2,1,0:T(8,128)(2,1)}, u32[]{:S(2)}) copy-start(bf16[64,8,512]{2,1,0:T(8,128)(2,1)} %param.21) | copy-start | bytes 1572868
  7.2 17.8 %copy-start.47 = (bf16[2,512,1024]{2,1,0:T(8,128)(2,1)S(1)}, bf16[2,512,1024]{2,1,0:T(8,128)(2,1)}, u32[]{:S(2)}) copy-start(bf16[2,512,1024]{2,1,0:T(8,128)(2,1)} %param.24) | copy-start | bytes 6291460
  7.2 53.3 %reduce-scatter.15.cloned.1.call-start = ((), (), s32[]{:S(2)}) async-start(), calls=%async_computation.8 | async-start | bytes 2621440
  28.7 1.4 copy-start.43
  28.7 2.0 copy-start.44
  28.7 2.6 copy-start.32
  28.7 3.2 %copy-start.33 = (f32[2,1024]{1,0:T(2,128)S(1)}, f32[2,1024]{1,0:T(2,128)}, u32[]{:S(2)}) copy-start(f32[2,1024]{1,0:T(2,128)} %param.35) | copy-start | bytes 24580
  28.7 3.7 %copy-start.26 = (bf16[2,4,768]{2,1,0:T(4,128)(2,1)S(1)}, bf16[2,4,768]{2,1,0:T(4,128)(2,1)}, u32[]{:S(2)}) copy-start(bf16[2,4,768]{2,1,0:T(4,128)(2,1)} %param.30) | copy-start | bytes 36868
  28.7 4.3 %copy-start.27 = (bf16[2,4,768]{2,1,0:T(4,128)(2,1)S(1)}, bf16[2,4,768]{2,1,0:T(4,128)(2,1)}, u32[]{:S(2)}) copy-start(bf16[2,4,768]{2,1,0:T(4,128)(2,1)} %param.31) | copy-start | bytes 36868
  28.8 4.9 %copy-start.14 = (f32[2,4,1024]{2,1,0:T(4,128)S(1)}, f32[2,4,1024]{2,1,0:T(4,128)}, u32[]{:S(2)}) copy-start(f32[2,4,1024]{2,1,0:T(4,128)} %param.26) | copy-start | bytes 98308
  28.8 5.5 %copy-start.11 = (bf16[2,16,3,1024]{3,1,2,0:T(8,128)(2,1)S(1)}, bf16[2,16,3,1024]{3,1,2,0:T(8,128)(2,1)}, u32[]{:S(2)}) copy-start(bf16[2,16,3,1024]{3,1,2,0:T(8,128)(2,1)} %param.37) | copy-start | bytes 589828
  28.8 73.8 %all-gather.3.cloned.1.call-start = ((), (), s32[]{:S(2)}) async-start(), calls=%async_computation.4 | async-start | bytes 1310720 | tf_op jit(solution)/shard_map/all_gather | solution.py:168
  29.4 32.5 %copy-start.28 = (pred[16,8]{0,1:T(8,128)(4,1)}, pred[16,8]{0,1:T(8,128)(4,1)S(1)}, u32[]{:S(2)}) copy-start(pred[16,8]{0,1:T(8,128)(4,1)S(1)} %iota_compare_fusion.1) | copy-start | bytes 388
  30.1 42.2 %copy-start.39 = (pred[8,8]{1,0:T(8,128)(4,1)}, pred[8,8]{1,0:T(8,128)(4,1)S(1)}, u32[]{:S(2)}) copy-start(pred[8,8]{1,0:T(8,128)(4,1)S(1)} %iota_compare_fusion) | copy-start | bytes 196
  30.7 41.6 %copy-start.38 = (f32[4]{0:T(128)}, f32[4]{0:T(128)S(1)}, u32[]{:S(2)}) copy-start(f32[4]{0:T(128)S(1)} %get-tuple-element.66) | copy-start | bytes 52
  60.5 3.0 copy-start.3
  63.4 1.7 copy-start.10
  63.4 1.7 copy-start.48
  65.6 16.6 %copy-start.6 = (bf16[4,16,8,256]{3,2,1,0:T(8,128)(2,1)}, bf16[4,16,8,256]{3,2,1,0:T(8,128)(2,1)S(1)}, u32[]{:S(2)}) copy-start(bf16[4,16,8,256]{3,2,1,0:T(8,128)(2,1)S(1)} %convolution_convert_fusion.9) | copy-start | bytes 786436
  73.5 8.7 %copy-start.15 = (f32[16,4,1]{0,1,2:T(4,128)}, f32[16,4,1]{0,1,2:T(4,128)S(1)}, u32[]{:S(2)}) copy-start(f32[16,4,1]{0,1,2:T(4,128)S(1)} %copy.232) | copy-start | bytes 772
  75.2 7.0 %copy-start.13 = (f32[16,4,8]{2,1,0:T(4,128)S(1)}, f32[16,4,8]{2,1,0:T(4,128)}, u32[]{:S(2)}) copy-start(f32[16,4,8]{2,1,0:T(4,128)} %copy-done.12) | copy-start | bytes 6148
  82.2 1.8 copy-start.23
  85.7 41.9 %reduce-scatter.11.cloned.1.call-start = ((), (), s32[]{:S(2)}) async-start(), calls=%async_computation.5 | async-start | bytes 655360 | tf_op jit(solution)/shard_map/reduce_scatter | solution.py:173
  105.6 49.1 %copy-start.42 = (f32[1,512]{1,0:T(1,128)S(1)}, f32[1,512]{1,0:T(1,128)}, u32[]{:S(2)}) copy-start(f32[1,512]{1,0:T(1,128)} %get-tuple-element.60) | copy-start | bytes 6148
  105.6 86.0 %reduce-scatter.17.cloned.1.call-start = ((), (), s32[]{:S(2)}) async-start(), calls=%async_computation.9 | async-start | bytes 2621440
  161.7 1.3 copy-start.34
  161.7 85.1 %all-gather.5.cloned.1.call-start = ((), (), s32[]{:S(2)}) async-start(), calls=%async_computation.6 | async-start | bytes 1310720 | tf_op jit(solution)/shard_map/all_gather | solution.py:168
  191.6 3.2 %copy-start.17 = (f32[1,1,1024]{2,1,0:T(1,128)S(1)}, f32[1,1,1024]{2,1,0:T(1,128)}, u32[]{:S(2)}) copy-start(f32[1,1,1024]{2,1,0:T(1,128)} %get-tuple-element.37) | copy-start | bytes 12292
  191.6 3.2 %copy-start.18 = (f32[1,1,1024]{2,1,0:T(1,128)S(1)}, f32[1,1,1024]{2,1,0:T(1,128)}, u32[]{:S(2)}) copy-start(f32[1,1,1024]{2,1,0:T(1,128)} %get-tuple-element.38) | copy-start | bytes 12292
  191.6 3.2 %copy-start.19 = (f32[1,1,1024]{2,1,0:T(1,128)S(1)}, f32[1,1,1024]{2,1,0:T(1,128)}, u32[]{:S(2)}) copy-start(f32[1,1,1024]{2,1,0:T(1,128)} %get-tuple-element.43) | copy-start | bytes 12292
  191.6 3.2 %copy-start.20 = (f32[1,1,1024]{2,1,0:T(1,128)S(1)}, f32[1,1,1024]{2,1,0:T(1,128)}, u32[]{:S(2)}) copy-start(f32[1,1,1024]{2,1,0:T(1,128)} %get-tuple-element.44) | copy-start | bytes 12292
  195.1 4.6 %copy-start.35 = (bf16[4,768,1,1]{1,0,2,3:T(4,128)(2,1)S(1)}, bf16[4,768,1,1]{1,0,2,3:T(4,128)(2,1)}, u32[]{:S(2)}) copy-start(bf16[4,768,1,1]{1,0,2,3:T(4,128)(2,1)} %get-tuple-element.49) | copy-start | bytes 18436
  195.3 2.9 copy-start.49
  196.7 4.8 %copy-start.1 = (bf16[4,16,8,256]{3,2,1,0:T(8,128)(2,1)}, bf16[4,16,8,256]{3,2,1,0:T(8,128)(2,1)S(1)}, u32[]{:S(2)}) copy-start(bf16[4,16,8,256]{3,2,1,0:T(8,128)(2,1)S(1)} %convolution_convert_fusion.8) | copy-start | bytes 786436
  198.2 5.2 %copy-start.4 = (bf16[4,16,8,256]{3,2,1,0:T(8,128)(2,1)}, bf16[4,16,8,256]{3,2,1,0:T(8,128)(2,1)S(1)}, u32[]{:S(2)}) copy-start(bf16[4,16,8,256]{3,2,1,0:T(8,128)(2,1)S(1)} %convolution_convert_fusion.7) | copy-start | bytes 786436
  198.2 3.4 %copy-start.36 = (bf16[4,768,1,1]{1,0,2,3:T(4,128)(2,1)S(1)}, bf16[4,768,1,1]{1,0,2,3:T(4,128)(2,1)}, u32[]{:S(2)}) copy-start(bf16[4,768,1,1]{1,0,2,3:T(4,128)(2,1)} %get-tuple-element.47) | copy-start | bytes 18436
  199.7 3.7 %copy-start.8 = (bf16[4,16,8,256]{3,2,1,0:T(8,128)(2,1)}, bf16[4,16,8,256]{3,2,1,0:T(8,128)(2,1)S(1)}, u32[]{:S(2)}) copy-start(bf16[4,16,8,256]{3,2,1,0:T(8,128)(2,1)S(1)} %convolution_convert_fusion.6) | copy-start | bytes 786436
  199.7 3.7 %copy-start.41 = (f32[4]{0:T(128)S(1)}, f32[4]{0:T(128)}, u32[]{:S(2)}) copy-start(f32[4]{0:T(128)} %get-tuple-element.63) | copy-start | bytes 52
  199.7 6.7 %copy-start.37 = (f32[4]{0:T(128)S(1)}, f32[4]{0:T(128)}, u32[]{:S(2)}) copy-start(f32[4]{0:T(128)} %get-tuple-element.65) | copy-start | bytes 52
  199.8 6.7 %copy-start.40 = (pred[8,8]{1,0:T(8,128)(4,1)S(1)}, pred[8,8]{1,0:T(8,128)(4,1)}, u32[]{:S(2)}) copy-start(pred[8,8]{1,0:T(8,128)(4,1)} %copy-done.39) | copy-start | bytes 196
  214.1 2.6 copy-start.31
  214.1 4.1 %copy-start.16 = (f32[16,4,1]{0,1,2:T(4,128)S(1)}, f32[16,4,1]{0,1,2:T(4,128)}, u32[]{:S(2)}) copy-start(f32[16,4,1]{0,1,2:T(4,128)} %copy-done.15) | copy-start | bytes 772
  214.2 4.1 %copy-start.25 = (f32[2,16,4]{1,2,0:T(4,128)S(1)}, f32[2,16,4]{1,2,0:T(4,128)}, u32[]{:S(2)}) copy-start(f32[2,16,4]{1,2,0:T(4,128)} %param.39) | copy-start | bytes 1540
  215.4 5.0 %copy-start.2 = (bf16[4,16,8,256]{3,2,1,0:T(8,128)(2,1)S(1)}, bf16[4,16,8,256]{3,2,1,0:T(8,128)(2,1)}, u32[]{:S(2)}) copy-start(bf16[4,16,8,256]{3,2,1,0:T(8,128)(2,1)} %copy-done.1) | copy-start | bytes 786436
  220.4 1.9 copy-start.22
  222.3 2.8 copy-start.9
  224.3 48.7 %reduce-scatter.13.cloned.1.call-start = ((), (), s32[]{:S(2)}) async-start(), calls=%async_computation.7 | async-start | bytes 655360 | tf_op jit(solution)/shard_map/reduce_scatter | solution.py:173
  225.1 10.9 %copy-start.7 = (bf16[4,16,8,256]{3,2,1,0:T(8,128)(2,1)S(1)}, bf16[4,16,8,256]{3,2,1,0:T(8,128)(2,1)}, u32[]{:S(2)}) copy-start(bf16[4,16,8,256]{3,2,1,0:T(8,128)(2,1)} %copy-done.6) | copy-start | bytes 786436
  (8 other events, 6.2 us)
Sparse Core Ops, SparseCore 0:
  28.9 31.4 reduce-scatter.14
  85.8 16.6 all-gather.2
  105.8 21.8 reduce-scatter.10
  161.9 29.7 reduce-scatter.16
  224.4 16.7 all-gather.4
  250.0 21.9 reduce-scatter.12
where the time goes:
time: 298 us; the launch traced here: 297 us
  waiting for transfers between devices  93 us (31%)
  matrix products  65.3 us (22%)
  blocking collectives  54.3 us (18%)
  other arithmetic  41.4 us (14%)
  local copies, waits for them, and re-layouts  27.7 us (9%)
  between operations  15 us (5%)
    unnamed x8, waiting for transfers between devices  54.4 us
    all_gather x2, blocking collectives, layer_step(): lax.all_gather(new_share, 'tp', axis=0, tiled=True)  31.1 us
    psum x2, blocking collectives, layer_step(): total_squares = lax.psum(partial_squares, 'dp')  23.2 us
    another operation x1, other arithmetic, per_device(): jnp.stack(memory_list)  23.1 us
    reduce_scatter x2, waiting for transfers between devices, layer_step(): lax.psum_scatter(flat_terms.astype(jnp.bfloat16), 'tp', scatter_dimension...  21.8 us
    dot_general x2, matrix products, recurrent_cell(): jnp.einsum('bhs,bhsd,bhse->bhde', update_weight, key_heads, value_heads)  21.7 us
    all_gather x2, waiting for transfers between devices, layer_step(): piece = lax.all_gather(mixed, 'dp', axis=0, tiled=True)  16.8 us
    dot_general x2, matrix products, recurrent_cell(): jnp.einsum('bhtd,bhde->bhte', query_heads, memory)  14 us
  transfers between devices with their start and end apart: 6, of which 4 were waited for; matrix products, arithmetic and copies ran while one was open for 17% of the time, Pallas kernels for 0%

commit v1 on v0

--- a/solution.py
+++ b/solution.py
@@ -130,7 +130,11 @@
     local_batch = live_counts.shape[0]
     floats = tokens.astype(jnp.float32)
     partial_squares = jnp.sum(floats * floats, axis=-1)
-    total_squares = lax.psum(partial_squares, "dp")
+
+    def _order_slabs(mine_x, axis_tag):
+        return lax.all_gather(mine_x, axis_tag).sum(axis=0)
+
+    total_squares = _order_slabs(partial_squares, "dp")
     normed = (floats * lax.rsqrt(total_squares / D + epsilon)[..., None] * gain).astype(
         jnp.bfloat16
     )

time: 298 us -> 289 us (0.970)
  blocking collectives: 54.3 us -> 42.6 us
    psum x2 -> x0, blocking collectives: 23.2 us -> none  [layer_step(): total_squares = lax.psum(partial_squares, 'dp')]
    all_gather x0 -> x2, blocking collectives: none -> 11.4 us  [_order_slabs(): return lax.all_gather(mine_x, axis_tag).sum(axis=0)]
    unnamed x110 -> x107, local copies, waits for them, and re-layouts: 11.9 us -> 11.9 us
  transfers between devices with their start and end apart: 6 -> 6, of which waited for: 4 -> 4; matrix products, arithmetic and copies ran while one was open for 17% -> 18% of each run, Pallas kernels for 0% -> 0%
where the time goes in v1:
time: 289 us; the launch traced here: 288 us
  waiting for transfers between devices  94.2 us (33%)
  matrix products  66.4 us (23%)
  blocking collectives  42.6 us (15%)
  other arithmetic  41.3 us (14%)
  local copies, waits for them, and re-layouts  28 us (10%)
  between operations  14.9 us (5%)
    unnamed x8, waiting for transfers between devices  55.6 us
    all_gather x2, blocking collectives, layer_step(): lax.all_gather(new_share, 'tp', axis=0, tiled=True)  31.2 us
    another operation x1, other arithmetic, per_device(): jnp.stack(memory_list)  23.1 us
    reduce_scatter x2, waiting for transfers between devices, layer_step(): lax.psum_scatter(flat_terms.astype(jnp.bfloat16), 'tp', scatter_dimension...  21.8 us
    dot_general x2, matrix products, recurrent_cell(): jnp.einsum('bhs,bhsd,bhse->bhde', update_weight, key_heads, value_heads)  21.7 us
    all_gather x2, waiting for transfers between devices, layer_step(): piece = lax.all_gather(mixed, 'dp', axis=0, tiled=True)  16.8 us
    dot_general x2, matrix products, recurrent_cell(): jnp.einsum('bhtd,bhde->bhte', query_heads, memory)  14 us
    unnamed x107, local copies, waits for them, and re-layouts  11.9 us
  transfers between devices with their start and end apart: 6, of which 4 were waited for; matrix products, arithmetic and copies ran while one was open for 18% of the time, Pallas kernels for 0%

profile of v1, /device:TPU:0, one launch (start us, length us, event | category | flops | bytes accessed | tf_op | source)
XLA Modules:
  0.0 287.9 jit_solution(6003115910297184096)
XLA Ops:
  7.2 1.4 fusion.162
  8.7 1.2 fusion.16
  10.0 6.2 %all-gather.1 = f32[4,64,8]{1,2,0:T(8,128)S(1)} all-gather(f32[1,64,8]{1,2,0:T(8,128)S(1)} %copy.257), channel_id=2, replica_groups=mesh['grp'=2,'tp'=4,'dp'=4] {'dp'}, dimensions={0}, use_global_device_ids=true | all-gather | bytes 10240 | tf_op jit(solution)/shard_map/all_gather | solution.py:135
  16.3 2.1 fusion.11
  19.7 2.5 copy.340
  27.8 27.5 %reduce-scatter.15.cloned.1.call-done = bf16[16,16384]{1,0:T(8,128)(2,1)} async-done(((bf16[64,16384]{1,0:T(8,128)(2,1)}), bf16[16,16384]{1,0:T(8,128)(2,1)}) %reduce-scatter.15.cloned.1.call-update) | async-done | bytes 524304
  55.3 1.4 copy.341
  57.0 0.9 reshape.327
  58.6 1.3 convolution_convert_fusion.10
  59.9 1.6 convolution_convert_fusion.9
  61.5 1.8 fusion.76
  63.3 1.8 fusion.77
  65.3 2.8 reduce_window_sum.17
  70.3 0.8 bitcast_multiply_fusion.6
  71.0 7.0 %fusion.4 = f32[16,4,8,256]{3,2,1,0:T(8,128)S(1)} fusion(f32[2,16,4,256,256]{4,3,2,1,0:T(8,128)} %param.38, bf16[4,16,8,256]{3,2,1,0:T(8,128)(2,1)S(1)} %convolution_convert_fusion.11), kind=kOutput, calls=%fused_computation.9 | convolution fusion | flops 67108864 | bytes 9175040 | tf_op jit(solution)/shard_map/bhtd,bhde->bhte/dot_general | solution.py:83
  78.0 1.4 fusion.108
  80.7 0.9 copy.273
  81.6 16.8 %all-gather.5.cloned.1.call-done = bf16[64,8,1024]{2,1,0:T(8,128)(2,1)} async-done(((bf16[16,8,1024]{2,1,0:T(8,128)(2,1)}), bf16[64,8,1024]{2,1,0:T(8,128)(2,1)}) %all-gather.5.cloned.1.call-update) | async-done | bytes 1048592 | tf_op jit(solution)/shard_map/all_gather | solution.py:172
  98.4 3.0 %convolution_convert_fusion.5 = bf16[512,512]{1,0:T(8,128)(2,1)} fusion(bf16[64,8,1024]{2,1,0:T(8,128)(2,1)} %all-gather.5.cloned.1.call-done, bf16[2,1024,512]{2,1,0:T(8,128)(2,1)} %param.36), kind=kOutput, calls=%fused_computation.29 | convolution fusion | flops 537133056 | bytes 2621440 | tf_op jit(solution)/shard_map/dot_general | solution.py:174
  101.7 21.8 %reduce-scatter.11.cloned.1.call-done = bf16[128,512]{1,0:T(8,128)(2,1)} async-done(((bf16[512,512]{1,0:T(8,128)(2,1)}), bf16[128,512]{1,0:T(8,128)(2,1)}) %reduce-scatter.11.cloned.1.call-update) | async-done | bytes 131088 | tf_op jit(solution)/shard_map/reduce_scatter | solution.py:177
  123.5 0.9 add_convert_fusion.1
  124.4 15.6 %all_gather.27 = bf16[512,512]{1,0:T(8,128)(2,1)S(1)} all-gather(bf16[128,512]{1,0:T(8,128)(2,1)S(1)} %add_convert_fusion.1), channel_id=1, replica_groups=mesh['grp'=2,'tp'=4,'dp'=4] {'tp'}, dimensions={0}, use_global_device_ids=true | all-gather | bytes 655360 | tf_op jit(solution)/shard_map/all_gather | solution.py:190
  140.4 5.2 %all_gather.29 = f32[4,64,8]{1,2,0:T(8,128)S(1)} all-gather(f32[1,64,8]{1,2,0:T(8,128)S(1)} %copy.274), channel_id=1, replica_groups=mesh['grp'=2,'tp'=4,'dp'=4] {'dp'}, dimensions={0}, use_global_device_ids=true | all-gather | bytes 10240 | tf_op jit(solution)/shard_map/all_gather | solution.py:135
  145.8 2.0 fusion.13
  147.8 2.0 fusion.12
  150.2 2.5 copy.342
  154.5 27.9 %reduce-scatter.17.cloned.1.call-done = bf16[16,16384]{1,0:T(8,128)(2,1)} async-done(((bf16[64,16384]{1,0:T(8,128)(2,1)}), bf16[16,16384]{1,0:T(8,128)(2,1)}) %reduce-scatter.17.cloned.1.call-update) | async-done | bytes 524304
  182.4 1.4 copy.343
  184.6 0.9 reshape.328
  186.1 1.4 convolution_convert_fusion.8
  187.5 1.4 convolution_convert_fusion.7
  189.0 1.5 convolution_convert_fusion.6
  190.5 1.8 fusion.74
  192.3 1.8 fusion.75
  194.4 2.8 reduce_window_sum.18
  197.8 7.1 %fusion = f32[16,4,8,256]{3,2,1,0:T(8,128)S(1)} fusion(f32[2,16,4,256,256]{4,3,2,1,0:T(8,128)} %param.38, bf16[4,16,8,256]{3,2,1,0:T(8,128)(2,1)} %copy-done.1), kind=kOutput, calls=%fused_computation.4 | convolution fusion | flops 67108864 | bytes 9175040 | tf_op jit(solution)/shard_map/bhtd,bhde->bhte/dot_general | solution.py:83
  204.9 1.2 gather_fusion
  206.1 1.2 gather_fusion.1
  209.4 1.7 bitcast_multiply_fusion.3
  211.2 1.5 fusion.109
  214.2 0.9 copy.288
  215.9 10.9 %fusion.3 = f32[1,16,4,256,256]{4,3,2,1,0:T(8,128)} fusion(f32[2,16,4,256,256]{4,3,2,1,0:T(8,128)} %param.38, f32[16,4]{1,0:T(8,128)S(1)} %copy.303, bf16[16,4,8,256]{3,2,0,1:T(8,128)(2,1)S(1)} %get-tuple-element.31, bf16[4,16,8,256]{3,2,1,0:T(8,128)(2,1)S(1)} %copy-done.9), kind=kOutput, calls=%fused_computation.7 | convolution fusion | flops 75497472 | bytes 34078976 | tf_op jit(solution)/shard_map/bhs,bhsd,bhse->bhde/dot_general | solution.py:95
  226.8 10.8 %fusion.7 = f32[1,16,4,256,256]{4,3,2,1,0:T(8,128)} fusion(f32[2,16,4,256,256]{4,3,2,1,0:T(8,128)} %param.38, f32[16,4]{1,0:T(8,128)S(1)} %copy.295, bf16[16,4,8,256]{3,2,0,1:T(8,128)(2,1)S(1)} %get-tuple-element.29, bf16[4,16,8,256]{3,2,1,0:T(8,128)(2,1)S(1)} %copy-done.7), kind=kOutput, calls=%fused_computation.12 | convolution fusion | flops 75497472 | bytes 34078976 | tf_op jit(solution)/shard_map/bhs,bhsd,bhse->bhde/dot_general | solution.py:95
  237.6 3.0 %convolution_convert_fusion.4 = bf16[512,512]{1,0:T(8,128)(2,1)} fusion(bf16[64,8,1024]{2,1,0:T(8,128)(2,1)} %all-gather.7.cloned.1.call-done, bf16[2,1024,512]{2,1,0:T(8,128)(2,1)} %param.36), kind=kOutput, calls=%fused_computation.28 | convolution fusion | flops 537133056 | bytes 2621440 | tf_op jit(solution)/shard_map/dot_general | solution.py:174
  240.7 23.1 %pad_maximum_fusion = f32[2,16,4,256,256]{4,3,2,1,0:T(8,128)} fusion(f32[1,16,4,256,256]{4,3,2,1,0:T(8,128)} %fusion.3, f32[1,16,4,256,256]{4,3,2,1,0:T(8,128)} %fusion.7), kind=kLoop, calls=%fused_computation.2 | loop fusion | flops 8388608 | bytes 67108864 | tf_op jit(solution)/shard_map/stack | solution.py:246
  263.7 0.9 add_convert_fusion
  264.7 15.6 %all_gather.31 = bf16[512,512]{1,0:T(8,128)(2,1)S(1)} all-gather(bf16[128,512]{1,0:T(8,128)(2,1)S(1)} %add_convert_fusion), channel_id=1, replica_groups=mesh['grp'=2,'tp'=4,'dp'=4] {'tp'}, dimensions={0}, use_global_device_ids=true | all-gather | bytes 655360 | tf_op jit(solution)/shard_map/all_gather | solution.py:190
  280.3 0.8 copy.441
  (202 shorter events, 20.6 us)
Async XLA Ops:
  7.2 11.3 %copy-start = (bf16[64,8,512]{2,1,0:T(8,128)(2,1)S(1)}, bf16[64,8,512]{2,1,0:T(8,128)(2,1)}, u32[]{:S(2)}) copy-start(bf16[64,8,512]{2,1,0:T(8,128)(2,1)} %param.21) | copy-start | bytes 1572868
  7.2 11.3 %copy-start.46 = (bf16[2,512,1024]{2,1,0:T(8,128)(2,1)S(1)}, bf16[2,512,1024]{2,1,0:T(8,128)(2,1)}, u32[]{:S(2)}) copy-start(bf16[2,512,1024]{2,1,0:T(8,128)(2,1)} %param.24) | copy-start | bytes 6291460
  7.2 48.1 %reduce-scatter.15.cloned.1.call-start = ((), (), s32[]{:S(2)}) async-start(), calls=%async_computation.8 | async-start | bytes 2621440
  22.2 1.4 copy-start.42
  22.2 2.0 copy-start.43
  22.2 2.5 copy-start.31
  22.2 3.1 %copy-start.32 = (f32[2,1024]{1,0:T(2,128)S(1)}, f32[2,1024]{1,0:T(2,128)}, u32[]{:S(2)}) copy-start(f32[2,1024]{1,0:T(2,128)} %param.35) | copy-start | bytes 24580
  22.2 3.7 %copy-start.25 = (bf16[2,4,768]{2,1,0:T(4,128)(2,1)S(1)}, bf16[2,4,768]{2,1,0:T(4,128)(2,1)}, u32[]{:S(2)}) copy-start(bf16[2,4,768]{2,1,0:T(4,128)(2,1)} %param.30) | copy-start | bytes 36868
  22.2 4.3 %copy-start.26 = (bf16[2,4,768]{2,1,0:T(4,128)(2,1)S(1)}, bf16[2,4,768]{2,1,0:T(4,128)(2,1)}, u32[]{:S(2)}) copy-start(bf16[2,4,768]{2,1,0:T(4,128)(2,1)} %param.31) | copy-start | bytes 36868
  22.3 4.9 %copy-start.13 = (f32[2,4,1024]{2,1,0:T(4,128)S(1)}, f32[2,4,1024]{2,1,0:T(4,128)}, u32[]{:S(2)}) copy-start(f32[2,4,1024]{2,1,0:T(4,128)} %param.26) | copy-start | bytes 98308
  22.3 5.5 %copy-start.10 = (bf16[2,16,3,1024]{3,1,2,0:T(8,128)(2,1)S(1)}, bf16[2,16,3,1024]{3,1,2,0:T(8,128)(2,1)}, u32[]{:S(2)}) copy-start(bf16[2,16,3,1024]{3,1,2,0:T(8,128)(2,1)} %param.37) | copy-start | bytes 589828
  22.3 76.1 %all-gather.5.cloned.1.call-start = ((), (), s32[]{:S(2)}) async-start(), calls=%async_computation.4 | async-start | bytes 1310720 | tf_op jit(solution)/shard_map/all_gather | solution.py:172
  22.9 33.9 %copy-start.27 = (pred[16,8]{0,1:T(8,128)(4,1)}, pred[16,8]{0,1:T(8,128)(4,1)S(1)}, u32[]{:S(2)}) copy-start(pred[16,8]{0,1:T(8,128)(4,1)S(1)} %iota_compare_fusion.1) | copy-start | bytes 388
  23.6 44.6 %copy-start.38 = (pred[8,8]{1,0:T(8,128)(4,1)}, pred[8,8]{1,0:T(8,128)(4,1)S(1)}, u32[]{:S(2)}) copy-start(pred[8,8]{1,0:T(8,128)(4,1)S(1)} %iota_compare_fusion) | copy-start | bytes 196
  24.2 44.0 %copy-start.37 = (f32[4]{0:T(128)}, f32[4]{0:T(128)S(1)}, u32[]{:S(2)}) copy-start(f32[4]{0:T(128)S(1)} %get-tuple-element.70) | copy-start | bytes 52
  55.3 3.0 %copy-start.3 = (bf16[2,4,256,256]{3,2,1,0:T(8,128)(2,1)S(1)}, bf16[2,4,256,256]{3,2,1,0:T(8,128)(2,1)}, u32[]{:S(2)}) copy-start(bf16[2,4,256,256]{3,2,1,0:T(8,128)(2,1)} %param.27) | copy-start | bytes 3145732
  61.5 16.5 %copy-start.6 = (bf16[4,16,8,256]{3,2,1,0:T(8,128)(2,1)}, bf16[4,16,8,256]{3,2,1,0:T(8,128)(2,1)S(1)}, u32[]{:S(2)}) copy-start(bf16[4,16,8,256]{3,2,1,0:T(8,128)(2,1)S(1)} %convolution_convert_fusion.9) | copy-start | bytes 786436
  69.4 8.6 %copy-start.14 = (f32[16,4,1]{0,1,2:T(4,128)}, f32[16,4,1]{0,1,2:T(4,128)S(1)}, u32[]{:S(2)}) copy-start(f32[16,4,1]{0,1,2:T(4,128)S(1)} %copy.293) | copy-start | bytes 772
  71.0 7.0 %copy-start.12 = (f32[16,4,8]{2,1,0:T(4,128)S(1)}, f32[16,4,8]{2,1,0:T(4,128)}, u32[]{:S(2)}) copy-start(f32[16,4,8]{2,1,0:T(4,128)} %copy-done.11) | copy-start | bytes 6148
  78.0 1.8 copy-start.22
  81.5 41.9 %reduce-scatter.11.cloned.1.call-start = ((), (), s32[]{:S(2)}) async-start(), calls=%async_computation.5 | async-start | bytes 655360 | tf_op jit(solution)/shard_map/reduce_scatter | solution.py:177
  101.5 44.3 %copy-start.41 = (f32[1,512]{1,0:T(1,128)S(1)}, f32[1,512]{1,0:T(1,128)}, u32[]{:S(2)}) copy-start(f32[1,512]{1,0:T(1,128)} %get-tuple-element.64) | copy-start | bytes 6148
  101.5 80.9 %reduce-scatter.17.cloned.1.call-start = ((), (), s32[]{:S(2)}) async-start(), calls=%async_computation.9 | async-start | bytes 2621440
  152.7 1.3 copy-start.33
  152.8 84.8 %all-gather.7.cloned.1.call-start = ((), (), s32[]{:S(2)}) async-start(), calls=%async_computation.6 | async-start | bytes 1310720 | tf_op jit(solution)/shard_map/all_gather | solution.py:172
  182.4 3.2 %copy-start.16 = (f32[1,1,1024]{2,1,0:T(1,128)S(1)}, f32[1,1,1024]{2,1,0:T(1,128)}, u32[]{:S(2)}) copy-start(f32[1,1,1024]{2,1,0:T(1,128)} %get-tuple-element.41) | copy-start | bytes 12292
  182.4 3.2 %copy-start.17 = (f32[1,1,1024]{2,1,0:T(1,128)S(1)}, f32[1,1,1024]{2,1,0:T(1,128)}, u32[]{:S(2)}) copy-start(f32[1,1,1024]{2,1,0:T(1,128)} %get-tuple-element.42) | copy-start | bytes 12292
  182.4 3.2 %copy-start.18 = (f32[1,1,1024]{2,1,0:T(1,128)S(1)}, f32[1,1,1024]{2,1,0:T(1,128)}, u32[]{:S(2)}) copy-start(f32[1,1,1024]{2,1,0:T(1,128)} %get-tuple-element.47) | copy-start | bytes 12292
  182.4 3.2 %copy-start.19 = (f32[1,1,1024]{2,1,0:T(1,128)S(1)}, f32[1,1,1024]{2,1,0:T(1,128)}, u32[]{:S(2)}) copy-start(f32[1,1,1024]{2,1,0:T(1,128)} %get-tuple-element.48) | copy-start | bytes 12292
  185.9 4.6 %copy-start.34 = (bf16[4,768,1,1]{1,0,2,3:T(4,128)(2,1)S(1)}, bf16[4,768,1,1]{1,0,2,3:T(4,128)(2,1)}, u32[]{:S(2)}) copy-start(bf16[4,768,1,1]{1,0,2,3:T(4,128)(2,1)} %get-tuple-element.53) | copy-start | bytes 18436
  186.1 2.9 copy-start.47
  187.5 4.8 %copy-start.1 = (bf16[4,16,8,256]{3,2,1,0:T(8,128)(2,1)}, bf16[4,16,8,256]{3,2,1,0:T(8,128)(2,1)S(1)}, u32[]{:S(2)}) copy-start(bf16[4,16,8,256]{3,2,1,0:T(8,128)(2,1)S(1)} %convolution_convert_fusion.8) | copy-start | bytes 786436
  189.0 5.2 %copy-start.4 = (bf16[4,16,8,256]{3,2,1,0:T(8,128)(2,1)}, bf16[4,16,8,256]{3,2,1,0:T(8,128)(2,1)S(1)}, u32[]{:S(2)}) copy-start(bf16[4,16,8,256]{3,2,1,0:T(8,128)(2,1)S(1)} %convolution_convert_fusion.7) | copy-start | bytes 786436
  189.0 3.4 %copy-start.35 = (bf16[4,768,1,1]{1,0,2,3:T(4,128)(2,1)S(1)}, bf16[4,768,1,1]{1,0,2,3:T(4,128)(2,1)}, u32[]{:S(2)}) copy-start(bf16[4,768,1,1]{1,0,2,3:T(4,128)(2,1)} %get-tuple-element.51) | copy-start | bytes 18436
  190.5 3.7 %copy-start.8 = (bf16[4,16,8,256]{3,2,1,0:T(8,128)(2,1)}, bf16[4,16,8,256]{3,2,1,0:T(8,128)(2,1)S(1)}, u32[]{:S(2)}) copy-start(bf16[4,16,8,256]{3,2,1,0:T(8,128)(2,1)S(1)} %convolution_convert_fusion.6) | copy-start | bytes 786436
  190.5 3.7 %copy-start.40 = (f32[4]{0:T(128)S(1)}, f32[4]{0:T(128)}, u32[]{:S(2)}) copy-start(f32[4]{0:T(128)} %get-tuple-element.67) | copy-start | bytes 52
  190.5 6.7 %copy-start.36 = (f32[4]{0:T(128)S(1)}, f32[4]{0:T(128)}, u32[]{:S(2)}) copy-start(f32[4]{0:T(128)} %get-tuple-element.69) | copy-start | bytes 52
  190.5 6.7 %copy-start.39 = (pred[8,8]{1,0:T(8,128)(4,1)S(1)}, pred[8,8]{1,0:T(8,128)(4,1)}, u32[]{:S(2)}) copy-start(pred[8,8]{1,0:T(8,128)(4,1)} %copy-done.38) | copy-start | bytes 196
  204.9 2.6 copy-start.30
  204.9 4.1 %copy-start.15 = (f32[16,4,1]{0,1,2:T(4,128)S(1)}, f32[16,4,1]{0,1,2:T(4,128)}, u32[]{:S(2)}) copy-start(f32[16,4,1]{0,1,2:T(4,128)} %copy-done.14) | copy-start | bytes 772
  204.9 4.1 %copy-start.24 = (f32[2,16,4]{1,2,0:T(4,128)S(1)}, f32[2,16,4]{1,2,0:T(4,128)}, u32[]{:S(2)}) copy-start(f32[2,16,4]{1,2,0:T(4,128)} %param.39) | copy-start | bytes 1540
  206.1 5.0 %copy-start.2 = (bf16[4,16,8,256]{3,2,1,0:T(8,128)(2,1)S(1)}, bf16[4,16,8,256]{3,2,1,0:T(8,128)(2,1)}, u32[]{:S(2)}) copy-start(bf16[4,16,8,256]{3,2,1,0:T(8,128)(2,1)} %copy-done.1) | copy-start | bytes 786436
  211.2 1.9 copy-start.21
  212.7 1.0 copy-start.5
  212.7 0.9 copy-start.20
  213.1 2.8 copy-start.9
  215.0 48.7 %reduce-scatter.13.cloned.1.call-start = ((), (), s32[]{:S(2)}) async-start(), calls=%async_computation.7 | async-start | bytes 655360 | tf_op jit(solution)/shard_map/reduce_scatter | solution.py:177
  215.9 10.9 %copy-start.7 = (bf16[4,16,8,256]{3,2,1,0:T(8,128)(2,1)S(1)}, bf16[4,16,8,256]{3,2,1,0:T(8,128)(2,1)}, u32[]{:S(2)}) copy-start(bf16[4,16,8,256]{3,2,1,0:T(8,128)(2,1)} %copy-done.6) | copy-start | bytes 786436
  (6 other events, 4.3 us)
Sparse Core Ops, SparseCore 0:
  22.4 32.8 reduce-scatter.14
  81.7 16.6 all-gather.4
  101.6 21.8 reduce-scatter.10
  152.9 29.4 reduce-scatter.16
  215.1 16.7 all-gather.6
  240.8 22.0 reduce-scatter.12
